TPU v7x, 32 devices: a whole 2x2x4 slice. The times are simulated.
32 devices in a mesh: grp: 2 (over y), tp: 4 (over z), dp: 4 (over x, core).
Axes of the slice: x: 2, y: 2, z: 4, core: 2. Of those that a mesh axis runs over, the one named last changes fastest.
Arguments:
- tokens: bfloat16 [64, 8, 4096], P(('grp', 'tp'), None, 'dp'), parts along dimension 0, may hold values from -6 to 6
- lengths: int32 [64], P('grp'), parts along dimension 0, may hold values from 1 to 8, 112 in all
- norm_gain: float32 [2, 4096], P(None, 'dp'), may hold values from 0.1 to 1.9
- w_recept: bfloat16 [2, 4096, 2048], P(None, 'dp', 'tp'), may hold values from -0.09375 to 0.09375
- w_key: bfloat16 [2, 4096, 2048], P(None, 'dp', 'tp'), may hold values from -0.09375 to 0.09375
- w_value: bfloat16 [2, 4096, 2048], P(None, 'dp', 'tp'), may hold values from -0.09375 to 0.09375
- w_decay: bfloat16 [2, 4096, 2048], P(None, 'dp', 'tp'), may hold values from -0.375 to 0.375
- w_rate: bfloat16 [2, 4096, 2048], P(None, 'dp', 'tp'), may hold values from -0.09375 to 0.09375
- w_gate: bfloat16 [2, 4096, 2048], P(None, 'dp', 'tp'), may hold values from -0.09375 to 0.09375
- w_out: bfloat16 [2, 2048, 4096], P(None, 'tp', 'dp'), may hold values from -0.125 to 0.125
- decay_base: float32 [2, 2048], P(None, 'tp'), may hold values from -4 to 3
- out_gain: float32 [2, 2048], P(None, 'tp'), may hold values from 0.1 to 1.9
- states: float32 [2, 64, 64, 2048], P(None, ('grp', 'dp'), None, 'tp'), parts along dimension 1, may hold values from -6 to 6
Outputs:
- stream_out: float32 [64, 8, 4096], P(('grp', 'tp'), None, 'dp'), parts along dimension 0
- new_states: float32 [2, 64, 64, 2048], P(None, ('grp', 'dp'), None, 'tp'), parts along dimension 1
There are 2 independent parts, one for each index of `grp`. A program takes and returns all parts, laid end to end along the dimension named above; an argument that names none is the same for every part. Nothing has to cross between parts.
Inputs may be any that keep to these rules, and one draw needn't show every extreme that they name: lengths[b] first tokens of sequence b are live; together they count 7 * 16 and the largest is 8.
All inputs are finite; a program needn't handle non-finite values.
Results may differ from a plain program's by a relative error of at most 0.0061.
Values may be sent and summed in bfloat16 or wider, within the bound.
A program may use at most 128 MiB of HBM per device.

v0:
```python
import jax
import jax.numpy as jnp
from jax import lax
from jax.sharding import PartitionSpec as P

D = 4096
HEAD = 64
BLOCKS = 2
group_eps = 0.00064
norm_eps = 1e-06
key_eps = 1e-06
decay_scale = 0.606531
highest = lax.Precision.HIGHEST


def mix_heads(
    state_in,
    recept,
    keys_in,
    values,
    decay_pre,
    rate_pre,
    gate_pre,
    base_shift,
    out_scale,
    live_mask,
    head_size,
):
    row_count, step_count, width_all = recept.shape
    head_count = width_all // head_size
    shape_heads = (row_count, step_count, head_count, head_size)
    decay_rate = jnp.exp(-decay_scale * jax.nn.sigmoid(decay_pre + base_shift)).reshape(shape_heads)
    learn_rate = jax.nn.sigmoid(rate_pre).reshape(shape_heads)
    key_heads = keys_in.reshape(shape_heads)
    unit_keys = key_heads * lax.rsqrt(
        jnp.sum(key_heads * key_heads, axis=3, keepdims=True) + key_eps
    )
    removal = unit_keys * learn_rate
    recept_heads = recept.reshape(shape_heads)
    value_heads = values.reshape(shape_heads)
    memory = state_in.reshape(row_count, head_size, head_count, head_size)
    outputs = []
    for position in range(step_count):
        seen_part = jnp.einsum("bihj,bhj->bhi", memory, unit_keys[:, position], precision=highest)
        updated = (
            memory * decay_rate[:, position][:, None, :, :]
            - jnp.swapaxes(seen_part, 1, 2)[:, :, :, None] * removal[:, position][:, None, :, :]
            + jnp.swapaxes(value_heads[:, position], 1, 2)[:, :, :, None]
            * key_heads[:, position][:, None, :, :]
        )
        memory = jnp.where(live_mask[:, position][:, None, None, None], updated, memory)
        outputs.append(
            jnp.einsum("bihj,bhj->bhi", memory, recept_heads[:, position], precision=highest)
        )
    readout = jnp.stack(outputs, axis=1)
    centered = readout - jnp.mean(readout, axis=3, keepdims=True)
    normed = centered * lax.rsqrt(jnp.mean(centered * centered, axis=3, keepdims=True) + group_eps)
    gated = normed.reshape(row_count, step_count, width_all) * out_scale * jax.nn.sigmoid(gate_pre)
    gated = jnp.where(live_mask[:, :, None], gated, 0.0)
    return (gated.astype(jnp.bfloat16), memory.reshape(row_count, head_size, width_all))


def body(
    tokens,
    lengths,
    norm_gain,
    w_recept,
    w_key,
    w_value,
    w_decay,
    w_rate,
    w_gate,
    w_out,
    decay_base,
    out_gain,
    states,
):
    horizon = tokens.shape[1]
    held_rows = states.shape[1]
    first_row = lax.axis_index("dp") * held_rows
    held_lengths = lax.dynamic_slice_in_dim(lengths, first_row, held_rows, 0)
    live_mask = jnp.arange(horizon, dtype=jnp.int32)[None, :] < held_lengths[:, None]
    current = tokens.astype(jnp.float32)
    finals = []
    for block_index in range(BLOCKS):
        gathered_in = lax.all_gather(current, "tp", axis=0, tiled=True)
        squares = jnp.sum(jnp.square(gathered_in), axis=2)
        total_squares = lax.psum_scatter(squares, "dp", scatter_dimension=0, tiled=True)
        inv_rms = lax.rsqrt(total_squares / D + norm_eps)
        scaled = (gathered_in * norm_gain[block_index]).astype(jnp.bfloat16)
        partials = tuple(
            (
                jnp.einsum(
                    "bsd,dc->bsc", scaled, weight[block_index], preferred_element_type=jnp.float32
                )
                for weight in (w_recept, w_key, w_value, w_decay, w_rate, w_gate)
            )
        )
        summed = lax.psum_scatter(partials, "dp", scatter_dimension=0, tiled=True)
        projected = [member * inv_rms[:, :, None] for member in summed]
        gated, final_state = mix_heads(
            states[block_index],
            projected[0],
            projected[1],
            projected[2],
            projected[3],
            projected[4],
            projected[5],
            decay_base[block_index],
            out_gain[block_index],
            live_mask,
            HEAD,
        )
        finals.append(final_state)
        all_rows = lax.all_gather(gated, "dp", axis=0, tiled=True)
        regrouped = lax.all_to_all(all_rows, "tp", split_axis=0, concat_axis=2, tiled=True)
        output = jnp.einsum(
            "bsc,cd->bsd",
            regrouped,
            lax.all_gather(w_out[block_index], "tp", axis=0, tiled=True),
            preferred_element_type=jnp.float32,
        )
        current = current + output
    return (current, jnp.stack(finals, axis=0))


def solution(mesh):
    in_specs = (
        P(("grp", "tp"), None, "dp"),
        P("grp"),
        P(None, "dp"),
        P(None, "dp", "tp"),
        P(None, "dp", "tp"),
        P(None, "dp", "tp"),
        P(None, "dp", "tp"),
        P(None, "dp", "tp"),
        P(None, "dp", "tp"),
        P(None, "tp", "dp"),
        P(None, "tp"),
        P(None, "tp"),
        P(None, ("grp", "dp"), None, "tp"),
    )
    out_specs = (P(("grp", "tp"), None, "dp"), P(None, ("grp", "dp"), None, "tp"))
    return jax.shard_map(body, mesh=mesh, in_specs=in_specs, out_specs=out_specs, check_vma=False)
```

profile of v0, /device:TPU:0, one launch (start us, length us, event | category | flops | bytes accessed | tf_op | source)
XLA Modules:
  0.0 758.3 jit_solution(8555726532389750007)
XLA Ops:
  10.4 30.4 %all-gather.7.cloned.1.call-done = f32[32,8,1024]{2,1,0:T(8,128)} async-done(((f32[8,8,1024]{2,1,0:T(8,128)}), f32[32,8,1024]{2,1,0:T(8,128)}) %all-gather.7.cloned.1.call-update) | async-done | bytes 1048592 | tf_op jit(solution)/shard_map/all_gather | solution.py:86
  54.3 3.2 fusion.112
  64.6 10.8 %all-reduce = f32[32,8]{1,0:T(8,128)S(1)} all-reduce(f32[32,8]{1,0:T(8,128)S(1)} %get-tuple-element.12), channel_id=5, replica_groups=mesh['grp'=2,'tp'=4,'dp'=4] {'dp'}, use_global_device_ids=true, to_apply=%region_2.0.clone | all-reduce | flops 256 | bytes 2048
  75.4 13.5 %reduce-scatter.15.cloned.1.call-done = f32[8,8,512]{2,1,0:T(8,128)} async-done(((f32[32,8,512]{2,1,0:T(8,128)}), f32[8,8,512]{2,1,0:T(8,128)}) %reduce-scatter.15.cloned.1.call-update) | async-done | bytes 131088 | tf_op jit(solution)/shard_map/reduce_scatter | solution.py:99
  88.9 24.0 %reduce-scatter.17.cloned.1.call-done = f32[8,8,512]{2,1,0:T(8,128)} async-done(((f32[32,8,512]{2,1,0:T(8,128)}), f32[8,8,512]{2,1,0:T(8,128)}) %reduce-scatter.17.cloned.1.call-update) | async-done | bytes 131088 | tf_op jit(solution)/shard_map/reduce_scatter | solution.py:99
  113.0 24.0 %reduce-scatter.19.cloned.1.call-done = f32[8,8,512]{2,1,0:T(8,128)} async-done(((f32[32,8,512]{2,1,0:T(8,128)}), f32[8,8,512]{2,1,0:T(8,128)}) %reduce-scatter.19.cloned.1.call-update) | async-done | bytes 131088 | tf_op jit(solution)/shard_map/reduce_scatter | solution.py:99
  137.0 24.0 %reduce-scatter.21.cloned.1.call-done = f32[8,8,512]{2,1,0:T(8,128)} async-done(((f32[32,8,512]{2,1,0:T(8,128)}), f32[8,8,512]{2,1,0:T(8,128)}) %reduce-scatter.21.cloned.1.call-update) | async-done | bytes 131088 | tf_op jit(solution)/shard_map/reduce_scatter | solution.py:99
  173.7 3.4 fusion.60
  178.2 3.3 add_select_fusion.14
  183.0 4.1 fusion.56
  190.3 5.1 add_select_fusion.13
  196.7 4.1 fusion.52
  204.0 5.8 add_select_fusion.12
  211.2 4.1 fusion.48
  218.4 7.1 add_select_fusion.11
  226.8 4.1 fusion.44
  234.1 8.6 %add_select_fusion.10 = f32[8,64,8,64]{3,2,1,0:T(8,128)S(1)} fusion(f32[8,8,64]{2,1,0:T(8,128)} %get-tuple-element.52, f32[8,64,8]{2,1,0:T(8,128)} %copy.40, f32[8,8,64]{2,1,0:T(8,128)} %get-tuple-element.36, f32[8,64,8]{2,1,0:T(8,128)} %bitcast.789, f32[8,8,64]{2,1,0:T(8,128)} %get-tuple-element.20, pred[8]{0:T(512)(128)(4,1)} %get-tuple-element.176, ...), kind=kLoop, calls=%fused_computation.21 | loop fusion | flops 9437184 | bytes 2588720 | tf_op jit(solution)/shard_map/jit(_where)/select_n | solution.py:51
  244.0 4.1 fusion.40
  251.2 10.0 %add_select_fusion.9 = f32[8,64,8,64]{3,2,1,0:T(8,128)S(1)} fusion(f32[8,8,64]{2,1,0:T(8,128)} %get-tuple-element.53, f32[8,64,8]{2,1,0:T(8,128)} %copy.41, f32[8,8,64]{2,1,0:T(8,128)} %get-tuple-element.37, f32[8,64,8]{2,1,0:T(8,128)} %bitcast.797, f32[8,8,64]{2,1,0:T(8,128)} %get-tuple-element.21, pred[8]{0:T(512)(128)(4,1)} %get-tuple-element.175, ...), kind=kLoop, calls=%fused_computation.20 | loop fusion | flops 11010048 | bytes 2670648 | tf_op jit(solution)/shard_map/jit(_where)/select_n | solution.py:51
  262.6 4.1 fusion.36
  268.2 5.2 fusion.62
  274.0 4.4 fusion.58
  279.1 4.4 fusion.54
  284.1 4.8 fusion.50
  289.5 4.4 fusion.46
  294.7 4.4 fusion.42
  299.7 4.2 fusion.38
  304.7 10.8 %add_select_fusion.8 = f32[8,64,8,64]{3,2,1,0:T(8,128)S(1)} fusion(f32[8,8,64]{2,1,0:T(8,128)} %get-tuple-element.54, f32[8,64,8]{2,1,0:T(8,128)S(1)} %copy-done.51, f32[8,8,64]{2,1,0:T(8,128)} %get-tuple-element.38, f32[8,64,8]{2,1,0:T(8,128)S(1)} %bitcast.804, f32[8,8,64]{2,1,0:T(8,128)} %get-tuple-element.22, pred[8]{0:T(512)(128)(4,1)S(1)} %copy-done.161, ...), kind=kLoop, calls=%fused_computation.19 | loop fusion | flops 12582912 | bytes 2752576 | tf_op jit(solution)/shard_map/jit(_where)/select_n | solution.py:51
  315.7 3.5 fusion.6
  324.7 5.8 all_gather.19
  330.4 13.7 %all_to_all.36 = bf16[32,8,512]{2,1,0:T(8,128)(2,1)S(1)} all-to-all(bf16[32,8,512]{2,1,0:T(8,128)(2,1)S(1)} %all_gather.19), channel_id=1, replica_groups=mesh['grp'=2,'tp'=4,'dp'=4] {'tp'}, dimensions={0} | all-to-all | bytes 524288 | tf_op jit(solution)/shard_map/all_to_all | solution.py:116
  344.3 3.7 fusion.64
  348.1 26.2 %all-gather.9.cloned.1.call-done = f32[32,8,1024]{2,1,0:T(8,128)} async-done(((f32[8,8,1024]{2,1,0:T(8,128)}), f32[32,8,1024]{2,1,0:T(8,128)}) %all-gather.9.cloned.1.call-update) | async-done | bytes 1048592 | tf_op jit(solution)/shard_map/all_gather | solution.py:86
  410.7 2.9 mul.1503
  433.1 2.9 mul.1481
  451.8 3.1 mul.1671
  492.1 8.9 %add_select_fusion.17 = f32[1,8,64,512]{3,2,1,0:T(8,128)} fusion(f32[1,8,64,512]{3,2,1,0:T(8,128)S(1)} %copy-done.48, f32[1,8,64,512]{3,2,1,0:T(8,128)} %mul.1722, f32[1,8,64,512]{3,2,1,0:T(8,128)} %mul.1715, f32[1,8,64,512]{3,2,1,0:T(8,128)} %mul.1711, f32[1,8,64,512]{3,2,1,0:T(8,128)} %mul.1704, f32[1,8,64,512]{3,2,1,0:T(8,128)} %mul.1700, ...), kind=kLoop, calls=%fused_computation.110 | loop fusion | flops 12582912 | bytes 19267648 | tf_op jit(solution)/shard_map/jit(_where)/select_n | solution.py:51
  501.0 10.7 %all-reduce.1 = f32[32,8]{1,0:T(8,128)S(1)} all-reduce(f32[32,8]{1,0:T(8,128)S(1)} %copy-done.146), channel_id=12, replica_groups=mesh['grp'=2,'tp'=4,'dp'=4] {'dp'}, use_global_device_ids=true, to_apply=%region_13.14.clone | all-reduce | flops 256 | bytes 2048
  522.4 3.5 fusion.34
  526.6 5.0 fusion.32
  532.7 3.6 add_select_fusion.6
  536.3 4.1 fusion.30
  540.4 4.1 fusion.28
  547.6 4.6 add_select_fusion.5
  553.5 4.1 fusion.24
  560.8 6.2 add_select_fusion.4
  568.4 4.1 fusion.20
  575.7 7.1 add_select_fusion.3
  584.1 4.1 fusion.16
  591.4 8.4 %add_select_fusion.2 = f32[8,64,8,64]{3,2,1,0:T(8,128)S(1)} fusion(f32[8,8,64]{2,1,0:T(8,128)} %get-tuple-element.100, f32[8,64,8]{2,1,0:T(8,128)} %copy.49, f32[8,8,64]{2,1,0:T(8,128)} %get-tuple-element.84, f32[8,64,8]{2,1,0:T(8,128)} %bitcast.793, f32[8,8,64]{2,1,0:T(8,128)} %get-tuple-element.68, pred[8]{0:T(512)(128)(4,1)} %get-tuple-element.176, ...), kind=kLoop, calls=%fused_computation.13 | loop fusion | flops 9437184 | bytes 2588720 | tf_op jit(solution)/shard_map/jit(_where)/select_n | solution.py:51
  601.2 4.1 fusion.12
  606.9 9.9 %add_select_fusion.1 = f32[8,64,8,64]{3,2,1,0:T(8,128)S(1)} fusion(f32[8,8,64]{2,1,0:T(8,128)} %get-tuple-element.101, f32[8,64,8]{2,1,0:T(8,128)} %copy.50, f32[8,8,64]{2,1,0:T(8,128)} %get-tuple-element.85, f32[8,64,8]{2,1,0:T(8,128)} %bitcast.800, f32[8,8,64]{2,1,0:T(8,128)} %get-tuple-element.69, pred[8]{0:T(512)(128)(4,1)} %get-tuple-element.175, ...), kind=kLoop, calls=%fused_computation.12 | loop fusion | flops 11010048 | bytes 2670648 | tf_op jit(solution)/shard_map/jit(_where)/select_n | solution.py:51
  618.1 4.1 fusion.8
  626.0 5.2 fusion.26
  631.8 4.4 fusion.22
  636.8 4.4 fusion.18
  642.0 4.6 fusion.14
  647.2 4.2 fusion.10
  652.3 10.7 %add_select_fusion = f32[8,64,8,64]{3,2,1,0:T(8,128)S(1)} fusion(f32[8,8,64]{2,1,0:T(8,128)} %get-tuple-element.102, f32[8,64,8]{2,1,0:T(8,128)} %copy.51, f32[8,8,64]{2,1,0:T(8,128)} %get-tuple-element.86, f32[8,64,8]{2,1,0:T(8,128)S(1)} %bitcast.806, f32[8,8,64]{2,1,0:T(8,128)} %get-tuple-element.70, pred[8]{0:T(512)(128)(4,1)S(1)} %copy-done.162, ...), kind=kLoop, calls=%fused_computation.11 | loop fusion | flops 12582912 | bytes 2752576 | tf_op jit(solution)/shard_map/jit(_where)/select_n | solution.py:51
  663.1 3.5 fusion.4
  672.1 6.2 all_gather.22
  678.3 4.4 all-to-all-start.1
  737.0 8.3 %add_select_fusion.16 = f32[1,8,64,512]{3,2,1,0:T(8,128)S(1)} fusion(f32[1,8,64,512]{3,2,1,0:T(8,128)} %mul.1814, f32[1,8,64,512]{3,2,1,0:T(8,128)} %mul.1810, f32[1,8,64,512]{3,2,1,0:T(8,128)} %mul.1803, f32[1,8,64,512]{3,2,1,0:T(8,128)} %mul.1799, f32[1,8,64,512]{3,2,1,0:T(8,128)} %mul.1792, f32[1,8,64,512]{3,2,1,0:T(8,128)} %mul.1788, ...), kind=kLoop, calls=%fused_computation.109 | loop fusion | flops 12582912 | bytes 19267648 | tf_op jit(solution)/shard_map/jit(_where)/select_n | solution.py:51
  747.9 3.7 fusion.67
  (651 shorter events, 283.4 us)
Async XLA Ops:
  7.2 35.1 %copy-start.171 = (bf16[2,1024,512]{2,1,0:T(8,128)(2,1)S(1)}, bf16[2,1024,512]{2,1,0:T(8,128)(2,1)}, u32[]{:S(2)}) copy-start(bf16[2,1024,512]{2,1,0:T(8,128)(2,1)} %param.19) | copy-start | bytes 6291460
  7.2 33.7 %all-gather.7.cloned.1.call-start = ((), (), s32[]{:S(2)}) async-start(), calls=%async_computation.14 | async-start | bytes 1310720 | tf_op jit(solution)/shard_map/all_gather | solution.py:86
  9.0 66.4 %reduce-scatter.13.cloned.1.call-start = ((), (), s32[]{:S(2)}) async-start(), calls=%async_computation.15 | async-start | bytes 655360 | tf_op jit(solution)/shard_map/reduce_scatter | solution.py:99
  43.6 45.4 %reduce-scatter.15.cloned.1.call-start = ((), (), s32[]{:S(2)}) async-start(), calls=%async_computation.16 | async-start | bytes 655360 | tf_op jit(solution)/shard_map/reduce_scatter | solution.py:99
  46.2 66.7 %reduce-scatter.17.cloned.1.call-start = ((), (), s32[]{:S(2)}) async-start(), calls=%async_computation.17 | async-start | bytes 655360 | tf_op jit(solution)/shard_map/reduce_scatter | solution.py:99
  47.6 89.4 %reduce-scatter.19.cloned.1.call-start = ((), (), s32[]{:S(2)}) async-start(), calls=%async_computation.18 | async-start | bytes 655360 | tf_op jit(solution)/shard_map/reduce_scatter | solution.py:99
  50.4 110.7 %reduce-scatter.21.cloned.1.call-start = ((), (), s32[]{:S(2)}) async-start(), calls=%async_computation.19 | async-start | bytes 655360 | tf_op jit(solution)/shard_map/reduce_scatter | solution.py:99
  51.7 271.9 %reduce-scatter.23.cloned.1.call-start = ((), (), s32[]{:S(2)}) async-start(), calls=%async_computation.20 | async-start | bytes 655360 | tf_op jit(solution)/shard_map/reduce_scatter | solution.py:99
  54.3 290.0 %all-gather.11.cloned.1.call-start = ((), (), s32[]{:S(2)}) async-start(), calls=%async_computation.28 | async-start | bytes 5242880 | tf_op jit(solution)/shard_map/all_gather | solution.py:120
  57.5 316.8 %all-gather.9.cloned.1.call-start = ((), (), s32[]{:S(2)}) async-start(), calls=%async_computation.21 | async-start | bytes 1310720 | tf_op jit(solution)/shard_map/all_gather | solution.py:86
  75.4 87.7 %copy-start.155 = (f32[8,8]{1,0:T(8,128)}, f32[8,8]{1,0:T(8,128)S(1)}, u32[]{:S(2)}) copy-start(f32[8,8]{1,0:T(8,128)S(1)} %fusion.109) | copy-start | bytes 772
  251.2 11.3 %copy-start.98 = (f32[8,1,8,64]{3,2,1,0:T(8,128)S(1)}, f32[8,1,8,64]{3,2,1,0:T(8,128)}, u32[]{:S(2)}) copy-start(f32[8,1,8,64]{3,2,1,0:T(8,128)} %get-tuple-element.134) | copy-start | bytes 49156
  268.2 10.8 %copy-start.13 = (f32[8,64,8,64]{3,2,1,0:T(8,128)S(1)}, f32[8,64,8,64]{3,2,1,0:T(8,128)}, u32[]{:S(2)}) copy-start(f32[8,64,8,64]{3,2,1,0:T(8,128)} %copy-done.12) | copy-start | bytes 3145732
  278.4 10.4 %copy-start.71 = (f32[8,8,1,64]{3,2,1,0:T(1,128)}, f32[8,8,1,64]{3,2,1,0:T(1,128)S(1)}, u32[]{:S(2)}) copy-start(f32[8,8,1,64]{3,2,1,0:T(1,128)S(1)} %fusion.58) | copy-start | bytes 49156
  279.0 10.4 %copy-start.20 = (f32[8,64,8,64]{3,2,1,0:T(8,128)S(1)}, f32[8,64,8,64]{3,2,1,0:T(8,128)}, u32[]{:S(2)}) copy-start(f32[8,64,8,64]{3,2,1,0:T(8,128)} %copy-done.19) | copy-start | bytes 3145732
  283.4 10.4 %copy-start.73 = (f32[8,8,1,64]{3,2,1,0:T(1,128)}, f32[8,8,1,64]{3,2,1,0:T(1,128)S(1)}, u32[]{:S(2)}) copy-start(f32[8,8,1,64]{3,2,1,0:T(1,128)S(1)} %fusion.54) | copy-start | bytes 49156
  284.1 10.4 %copy-start.2 = (f32[8,64,8,64]{3,2,1,0:T(8,128)S(1)}, f32[8,64,8,64]{3,2,1,0:T(8,128)}, u32[]{:S(2)}) copy-start(f32[8,64,8,64]{3,2,1,0:T(8,128)} %copy-done.1) | copy-start | bytes 3145732
  289.5 10.2 %copy-start.4 = (f32[8,64,8,64]{3,2,1,0:T(8,128)S(1)}, f32[8,64,8,64]{3,2,1,0:T(8,128)}, u32[]{:S(2)}) copy-start(f32[8,64,8,64]{3,2,1,0:T(8,128)} %copy-done.3) | copy-start | bytes 3145732
  299.0 16.5 %copy-start.85 = (f32[8,8,1,64]{3,2,1,0:T(1,128)}, f32[8,8,1,64]{3,2,1,0:T(1,128)S(1)}, u32[]{:S(2)}) copy-start(f32[8,8,1,64]{3,2,1,0:T(1,128)S(1)} %fusion.42) | copy-start | bytes 49156
  304.7 10.9 %copy-start.93 = (f32[8,1,8,64]{3,2,1,0:T(8,128)S(1)}, f32[8,1,8,64]{3,2,1,0:T(8,128)}, u32[]{:S(2)}) copy-start(f32[8,1,8,64]{3,2,1,0:T(8,128)} %get-tuple-element.150) | copy-start | bytes 49156
  322.1 22.2 %copy-start.64 = (bf16[8,8,1024]{2,1,0:T(8,128)(2,1)S(1)}, bf16[8,8,1024]{2,1,0:T(8,128)(2,1)}, u32[]{:S(2)}) copy-start(bf16[8,8,1024]{2,1,0:T(8,128)(2,1)} %param.13) | copy-start | bytes 393220
  344.3 30.0 %copy-start.160 = (f32[1,1024]{1,0:T(1,128)S(1)}, f32[1,1024]{1,0:T(1,128)}, u32[]{:S(2)}) copy-start(f32[1,1024]{1,0:T(1,128)} %get-tuple-element.158) | copy-start | bytes 12292
  348.0 163.7 %reduce-scatter.25.cloned.1.call-start = ((), (), s32[]{:S(2)}) async-start(), calls=%async_computation.22 | async-start | bytes 655360 | tf_op jit(solution)/shard_map/reduce_scatter | solution.py:99
  378.8 132.9 %reduce-scatter.27.cloned.1.call-start = ((), (), s32[]{:S(2)}) async-start(), calls=%async_computation.23 | async-start | bytes 655360 | tf_op jit(solution)/shard_map/reduce_scatter | solution.py:99
  381.4 130.4 %reduce-scatter.29.cloned.1.call-start = ((), (), s32[]{:S(2)}) async-start(), calls=%async_computation.24 | async-start | bytes 655360 | tf_op jit(solution)/shard_map/reduce_scatter | solution.py:99
  383.9 127.9 %reduce-scatter.31.cloned.1.call-start = ((), (), s32[]{:S(2)}) async-start(), calls=%async_computation.25 | async-start | bytes 655360 | tf_op jit(solution)/shard_map/reduce_scatter | solution.py:99
  386.5 125.4 %reduce-scatter.33.cloned.1.call-start = ((), (), s32[]{:S(2)}) async-start(), calls=%async_computation.26 | async-start | bytes 655360 | tf_op jit(solution)/shard_map/reduce_scatter | solution.py:99
  389.0 282.0 %reduce-scatter.35.cloned.1.call-start = ((), (), s32[]{:S(2)}) async-start(), calls=%async_computation.27 | async-start | bytes 655360 | tf_op jit(solution)/shard_map/reduce_scatter | solution.py:99
  391.6 356.2 %all-gather.13.cloned.1.call-start = ((), (), s32[]{:S(2)}) async-start(), calls=%async_computation.29 | async-start | bytes 5242880 | tf_op jit(solution)/shard_map/all_gather | solution.py:120
  475.4 12.2 %copy-start.113 = (f32[8,1,8,64]{3,2,1,0:T(8,128)S(1)}, f32[8,1,8,64]{3,2,1,0:T(8,128)}, u32[]{:S(2)}) copy-start(f32[8,1,8,64]{3,2,1,0:T(8,128)} %get-tuple-element.59) | copy-start | bytes 49156
  475.4 12.9 %copy-start.121 = (f32[8,1,8,64]{3,2,1,0:T(8,128)S(1)}, f32[8,1,8,64]{3,2,1,0:T(8,128)}, u32[]{:S(2)}) copy-start(f32[8,1,8,64]{3,2,1,0:T(8,128)} %get-tuple-element.43) | copy-start | bytes 49156
  475.4 13.8 %copy-start.112 = (f32[8,1,8,64]{3,2,1,0:T(8,128)S(1)}, f32[8,1,8,64]{3,2,1,0:T(8,128)}, u32[]{:S(2)}) copy-start(f32[8,1,8,64]{3,2,1,0:T(8,128)} %get-tuple-element.60) | copy-start | bytes 49156
  475.4 13.9 %copy-start.120 = (f32[8,1,8,64]{3,2,1,0:T(8,128)S(1)}, f32[8,1,8,64]{3,2,1,0:T(8,128)}, u32[]{:S(2)}) copy-start(f32[8,1,8,64]{3,2,1,0:T(8,128)} %get-tuple-element.44) | copy-start | bytes 49156
  475.4 14.8 %copy-start.111 = (f32[8,1,8,64]{3,2,1,0:T(8,128)S(1)}, f32[8,1,8,64]{3,2,1,0:T(8,128)}, u32[]{:S(2)}) copy-start(f32[8,1,8,64]{3,2,1,0:T(8,128)} %get-tuple-element.61) | copy-start | bytes 49156
  475.4 14.8 %copy-start.119 = (f32[8,1,8,64]{3,2,1,0:T(8,128)S(1)}, f32[8,1,8,64]{3,2,1,0:T(8,128)}, u32[]{:S(2)}) copy-start(f32[8,1,8,64]{3,2,1,0:T(8,128)} %get-tuple-element.45) | copy-start | bytes 49156
  475.4 15.7 %copy-start.110 = (f32[8,1,8,64]{3,2,1,0:T(8,128)S(1)}, f32[8,1,8,64]{3,2,1,0:T(8,128)}, u32[]{:S(2)}) copy-start(f32[8,1,8,64]{3,2,1,0:T(8,128)} %get-tuple-element.46) | copy-start | bytes 49156
  475.4 15.8 %copy-start.118 = (f32[8,1,8,64]{3,2,1,0:T(8,128)S(1)}, f32[8,1,8,64]{3,2,1,0:T(8,128)}, u32[]{:S(2)}) copy-start(f32[8,1,8,64]{3,2,1,0:T(8,128)} %get-tuple-element.30) | copy-start | bytes 49156
  475.4 16.7 %copy-start.48 = (f32[1,8,64,512]{3,2,1,0:T(8,128)S(1)}, f32[1,8,64,512]{3,2,1,0:T(8,128)}, u32[]{:S(2)}) copy-start(f32[1,8,64,512]{3,2,1,0:T(8,128)} %mul.1726) | copy-start | bytes 3145732
  492.1 19.7 %copy-start.167 = (f32[1,512]{1,0:T(1,128)S(1)}, f32[1,512]{1,0:T(1,128)}, u32[]{:S(2)}) copy-start(f32[1,512]{1,0:T(1,128)} %get-tuple-element.167) | copy-start | bytes 6148
  606.9 11.2 %copy-start.97 = (f32[8,1,8,64]{3,2,1,0:T(8,128)S(1)}, f32[8,1,8,64]{3,2,1,0:T(8,128)}, u32[]{:S(2)}) copy-start(f32[8,1,8,64]{3,2,1,0:T(8,128)} %get-tuple-element.110) | copy-start | bytes 49156
  626.0 10.8 %copy-start.22 = (f32[8,64,8,64]{3,2,1,0:T(8,128)S(1)}, f32[8,64,8,64]{3,2,1,0:T(8,128)}, u32[]{:S(2)}) copy-start(f32[8,64,8,64]{3,2,1,0:T(8,128)} %copy-done.21) | copy-start | bytes 3145732
  636.8 10.4 %copy-start.8 = (f32[8,64,8,64]{3,2,1,0:T(8,128)S(1)}, f32[8,64,8,64]{3,2,1,0:T(8,128)}, u32[]{:S(2)}) copy-start(f32[8,64,8,64]{3,2,1,0:T(8,128)} %copy-done.7) | copy-start | bytes 3145732
  641.8 10.3 %copy-start.25 = (f32[8,8,1,64]{1,3,0,2:T(8,128)S(1)}, f32[8,8,1,64]{1,3,0,2:T(8,128)}, u32[]{:S(2)}) copy-start(f32[8,8,1,64]{1,3,0,2:T(8,128)} %copy.112) | copy-start | bytes 49156
  641.8 10.3 %copy-start.29 = (f32[8,64,8]{2,1,0:T(8,128)S(1)}, f32[8,64,8]{2,1,0:T(8,128)}, u32[]{:S(2)}) copy-start(f32[8,64,8]{2,1,0:T(8,128)} %copy.47) | copy-start | bytes 49156
  641.8 10.3 %copy-start.31 = (f32[8,8,1,64]{1,3,0,2:T(8,128)S(1)}, f32[8,8,1,64]{1,3,0,2:T(8,128)}, u32[]{:S(2)}) copy-start(f32[8,8,1,64]{1,3,0,2:T(8,128)} %copy.117) | copy-start | bytes 49156
  641.9 10.2 %copy-start.35 = (f32[8,64,8]{2,1,0:T(8,128)S(1)}, f32[8,64,8]{2,1,0:T(8,128)}, u32[]{:S(2)}) copy-start(f32[8,64,8]{2,1,0:T(8,128)} %copy.48) | copy-start | bytes 49156
  641.9 10.2 %copy-start.37 = (f32[8,8,1,64]{1,3,0,2:T(8,128)S(1)}, f32[8,8,1,64]{1,3,0,2:T(8,128)}, u32[]{:S(2)}) copy-start(f32[8,8,1,64]{1,3,0,2:T(8,128)} %copy.122) | copy-start | bytes 49156
  641.9 10.2 %copy-start.42 = (f32[8,64,8]{2,1,0:T(8,128)S(1)}, f32[8,64,8]{2,1,0:T(8,128)}, u32[]{:S(2)}) copy-start(f32[8,64,8]{2,1,0:T(8,128)} %copy.49) | copy-start | bytes 49156
  641.9 10.2 %copy-start.43 = (f32[8,8,1,64]{1,3,0,2:T(8,128)S(1)}, f32[8,8,1,64]{1,3,0,2:T(8,128)}, u32[]{:S(2)}) copy-start(f32[8,8,1,64]{1,3,0,2:T(8,128)} %copy.127) | copy-start | bytes 49156
  641.9 10.2 %copy-start.46 = (f32[8,64,8]{2,1,0:T(8,128)S(1)}, f32[8,64,8]{2,1,0:T(8,128)}, u32[]{:S(2)}) copy-start(f32[8,64,8]{2,1,0:T(8,128)} %copy.50) | copy-start | bytes 49156
  641.9 10.2 %copy-start.47 = (f32[8,8,1,64]{1,3,0,2:T(8,128)S(1)}, f32[8,8,1,64]{1,3,0,2:T(8,128)}, u32[]{:S(2)}) copy-start(f32[8,8,1,64]{1,3,0,2:T(8,128)} %copy.132) | copy-start | bytes 49156
  641.9 10.2 %copy-start.53 = (f32[8,8,1,64]{1,3,0,2:T(8,128)S(1)}, f32[8,8,1,64]{1,3,0,2:T(8,128)}, u32[]{:S(2)}) copy-start(f32[8,8,1,64]{1,3,0,2:T(8,128)} %copy.137) | copy-start | bytes 49156
  641.9 10.2 %copy-start.55 = (f32[8,8,64]{2,1,0:T(8,128)S(1)}, f32[8,8,64]{2,1,0:T(8,128)}, u32[]{:S(2)}) copy-start(f32[8,8,64]{2,1,0:T(8,128)} %get-tuple-element.80) | copy-start | bytes 49156
  641.9 10.2 %copy-start.57 = (f32[8,8,64]{2,1,0:T(8,128)S(1)}, f32[8,8,64]{2,1,0:T(8,128)}, u32[]{:S(2)}) copy-start(f32[8,8,64]{2,1,0:T(8,128)} %get-tuple-element.64) | copy-start | bytes 49156
  641.9 10.2 %copy-start.59 = (f32[8,8,64]{2,1,0:T(8,128)S(1)}, f32[8,8,64]{2,1,0:T(8,128)}, u32[]{:S(2)}) copy-start(f32[8,8,64]{2,1,0:T(8,128)} %get-tuple-element.97) | copy-start | bytes 49156
  642.0 10.2 %copy-start.61 = (f32[8,8,64]{2,1,0:T(8,128)S(1)}, f32[8,8,64]{2,1,0:T(8,128)}, u32[]{:S(2)}) copy-start(f32[8,8,64]{2,1,0:T(8,128)} %get-tuple-element.81) | copy-start | bytes 49156
  642.0 10.2 %copy-start.63 = (f32[8,8,64]{2,1,0:T(8,128)S(1)}, f32[8,8,64]{2,1,0:T(8,128)}, u32[]{:S(2)}) copy-start(f32[8,8,64]{2,1,0:T(8,128)} %get-tuple-element.65) | copy-start | bytes 49156
  642.0 10.2 %copy-start.148 = (pred[8]{0:T(512)(128)(4,1)S(1)}, pred[8]{0:T(512)(128)(4,1)}, u32[]{:S(2)}) copy-start(pred[8]{0:T(512)(128)(4,1)} %get-tuple-element.177) | copy-start | bytes 28
  642.0 10.2 %copy-start.151 = (pred[8]{0:T(512)(128)(4,1)S(1)}, pred[8]{0:T(512)(128)(4,1)}, u32[]{:S(2)}) copy-start(pred[8]{0:T(512)(128)(4,1)} %get-tuple-element.176) | copy-start | bytes 28
  642.0 10.2 %copy-start.158 = (pred[8]{0:T(512)(128)(4,1)S(1)}, pred[8]{0:T(512)(128)(4,1)}, u32[]{:S(2)}) copy-start(pred[8]{0:T(512)(128)(4,1)} %get-tuple-element.175) | copy-start | bytes 28
  642.0 10.2 %copy-start.162 = (pred[8]{0:T(512)(128)(4,1)S(1)}, pred[8]{0:T(512)(128)(4,1)}, u32[]{:S(2)}) copy-start(pred[8]{0:T(512)(128)(4,1)} %get-tuple-element.174) | copy-start | bytes 28
  646.6 16.4 %copy-start.87 = (f32[8,8,1,64]{3,2,1,0:T(1,128)}, f32[8,8,1,64]{3,2,1,0:T(1,128)S(1)}, u32[]{:S(2)}) copy-start(f32[8,8,1,64]{3,2,1,0:T(1,128)S(1)} %fusion.14) | copy-start | bytes 49156
  652.3 10.8 %copy-start.94 = (f32[8,1,8,64]{3,2,1,0:T(8,128)S(1)}, f32[8,1,8,64]{3,2,1,0:T(8,128)}, u32[]{:S(2)}) copy-start(f32[8,1,8,64]{3,2,1,0:T(8,128)} %get-tuple-element.126) | copy-start | bytes 49156
  678.3 68.5 %all-to-all-start.1 = ((bf16[32,8,512]{2,1,0:T(8,128)(2,1)}), bf16[32,8,512]{2,1,0:T(8,128)(2,1)}, u32[]{:S(2)}, u32[]{:S(2)}) async-start(bf16[32,8,512]{2,1,0:T(8,128)(2,1)} %all_gather.22), calls=%async_computation.13 | async-start | bytes 524288 | tf_op jit(solution)/shard_map/all_to_all | solution.py:116
  (129 other events, 662.1 us)
Sparse Core Ops, SparseCore 0:
  10.1 30.6 all-gather.6
  43.7 20.9 reduce-scatter.12
  67.2 21.6 reduce-scatter.14
  91.3 21.6 reduce-scatter.16
  115.3 21.6 reduce-scatter.18
  139.3 21.6 reduce-scatter.20
  163.5 21.6 reduce-scatter.22
  186.8 80.7 all-gather.10
  348.2 26.1 all-gather.8
  379.0 20.9 reduce-scatter.24
  402.5 21.6 reduce-scatter.26
  426.5 21.6 reduce-scatter.28
  450.7 21.6 reduce-scatter.30
  474.7 21.6 reduce-scatter.32
  498.8 21.6 reduce-scatter.34
  521.9 80.7 all-gather.12
where the time goes:
time: 768 us; the launch traced here: 758 us
  local copies, waits for them, and re-layouts  245 us (32%)
  matrix products  160 us (21%)
  waiting for transfers between devices  143 us (19%)
  other arithmetic  140 us (18%)
  blocking collectives  47.2 us (6%)
  between operations  17.2 us (2%)
    select_n x18, other arithmetic, mix_heads(): jnp.where(live_mask[:, position][:, None, None, None], updated, memory)  121 us
    reduce_scatter x12, waiting for transfers between devices, body(): summed = lax.psum_scatter(partials, 'dp', scatter_dimension=0, tiled=True)  85.8 us
    mul x48, local copies, waits for them, and re-layouts, mix_heads(): jnp.swapaxes(seen_part, 1, 2)[:, :, :, None]  73.4 us
    mul x48, local copies, waits for them, and re-layouts, mix_heads(): jnp.swapaxes(value_heads[:, position], 1, 2)[:, :, :, None]  71 us
    dot_general x16, matrix products, mix_heads(): jnp.einsum('bihj,bhj->bhi', memory, recept_heads[:, position], precision=...  68.7 us
    dot_general x14, matrix products, mix_heads(): jnp.einsum('bihj,bhj->bhi', memory, unit_keys[:, position], precision=hig...  57.4 us
    all_gather x2, waiting for transfers between devices, body(): gathered_in = lax.all_gather(current, 'tp', axis=0, tiled=True)  56.7 us
    dot_general x12, matrix products, body(): jnp.einsum('bsd,dc->bsc', scaled, weight[block_index], preferred_element_...  26.4 us
  transfers between devices with their start and end apart: 17, of which 6 were waited for; matrix products, arithmetic and copies ran while one was open for 68% of the time, Pallas kernels for 0%

commit v1 on v0

--- a/solution.py
+++ b/solution.py
@@ -83,7 +83,14 @@
     current = tokens.astype(jnp.float32)
     finals = []
     for block_index in range(BLOCKS):
-        gathered_in = lax.all_gather(current, "tp", axis=0, tiled=True)
+        size = lax.axis_size("tp")
+        right = [(i, (i + 1) % size) for i in range(size)]
+        parts = [current]
+        for reach in range(1, size):
+            parts = [lax.ppermute(parts[0], "tp", right), *parts]
+        full = jnp.concatenate(parts, axis=0)
+        turn = (lax.axis_index("tp") + 1) * parts[-1].shape[0]
+        gathered_in = jnp.roll(full, turn, axis=0)
         squares = jnp.sum(jnp.square(gathered_in), axis=2)
         total_squares = lax.psum_scatter(squares, "dp", scatter_dimension=0, tiled=True)
         inv_rms = lax.rsqrt(total_squares / D + norm_eps)

time: 768 us -> 760 us (0.990)
  waiting for transfers between devices: 143 us -> 133 us
    all_gather x2 -> x0, waiting for transfers between devices: 56.7 us -> none  [body(): gathered_in = lax.all_gather(current, 'tp', axis=0, tiled=True)]
    ppermute x0 -> x6, waiting for transfers between devices: none -> 48.9 us  [body(): parts = [lax.ppermute(parts[0], 'tp', right), *parts]]
    unnamed x367 -> x371, local copies, waits for them, and re-layouts: 26.2 us -> 26.2 us
  transfers between devices with their start and end apart: 17 -> 21, of which waited for: 6 -> 10; matrix products, arithmetic and copies ran while one was open for 68% -> 68% of each run, Pallas kernels for 0% -> 0%
where the time goes in v1:
time: 760 us; the launch traced here: 750 us
  local copies, waits for them, and re-layouts  245 us (32%)
  matrix products  158 us (21%)
  other arithmetic  138 us (18%)
  waiting for transfers between devices  133 us (18%)
  blocking collectives  47.4 us (6%)
  between operations  19 us (2%)
  starting transfers between devices  8.41 us (1%)
    select_n x18, other arithmetic, mix_heads(): jnp.where(live_mask[:, position][:, None, None, None], updated, memory)  121 us
    reduce_scatter x12, waiting for transfers between devices, body(): summed = lax.psum_scatter(partials, 'dp', scatter_dimension=0, tiled=True)  83.7 us
    mul x48, local copies, waits for them, and re-layouts, mix_heads(): jnp.swapaxes(seen_part, 1, 2)[:, :, :, None]  73.3 us
    mul x48, local copies, waits for them, and re-layouts, mix_heads(): jnp.swapaxes(value_heads[:, position], 1, 2)[:, :, :, None]  71 us
    dot_general x16, matrix products, mix_heads(): jnp.einsum('bihj,bhj->bhi', memory, recept_heads[:, position], precision=...  68.7 us
    dot_general x14, matrix products, mix_heads(): jnp.einsum('bihj,bhj->bhi', memory, unit_keys[:, position], precision=hig...  57.4 us
    ppermute x6, waiting for transfers between devices, body(): parts = [lax.ppermute(parts[0], 'tp', right), *parts]  48.9 us
    unnamed x371, local copies, waits for them, and re-layouts  26.2 us
  transfers between devices with their start and end apart: 21, of which 10 were waited for; matrix products, arithmetic and copies ran while one was open for 68% of the time, Pallas kernels for 0%

profile of v1, /device:TPU:0, one launch (start us, length us, event | category | flops | bytes accessed | tf_op | source)
XLA Modules:
  0.0 750.0 jit_solution(12059045723461581862)
XLA Ops:
  12.2 8.3 %collective-permute-done = f32[8,8,1024]{2,1,0:T(8,128)S(1)} collective-permute-done((f32[8,8,1024]{2,1,0:T(8,128)S(1)}, f32[8,8,1024]{2,1,0:T(8,128)S(1)}, u32[]{:S(2)}, u32[]{:S(2)}) %collective-permute-start) | collective-permute-done | bytes 262176 | tf_op jit(solution)/shard_map/ppermute | solution.py:90
  20.6 9.3 %collective-permute-done.1 = f32[8,8,1024]{2,1,0:T(8,128)S(1)} collective-permute-done((f32[8,8,1024]{2,1,0:T(8,128)S(1)}, f32[8,8,1024]{2,1,0:T(8,128)S(1)}, u32[]{:S(2)}, u32[]{:S(2)}) %collective-permute-start.1) | collective-permute-done | bytes 262176 | tf_op jit(solution)/shard_map/ppermute | solution.py:90
  31.2 7.0 collective-permute-done.2
  51.1 3.2 fusion.128
  61.5 11.2 %all-reduce = f32[32,8]{1,0:T(8,128)S(1)} all-reduce(f32[32,8]{1,0:T(8,128)S(1)} %get-tuple-element.9), channel_id=5, replica_groups=mesh['grp'=2,'tp'=4,'dp'=4] {'dp'}, use_global_device_ids=true, to_apply=%region_2.4.clone | all-reduce | flops 256 | bytes 2048
  72.7 11.3 %reduce-scatter.15.cloned.1.call-done = f32[8,8,512]{2,1,0:T(8,128)} async-done(((f32[32,8,512]{2,1,0:T(8,128)}), f32[8,8,512]{2,1,0:T(8,128)}) %reduce-scatter.15.cloned.1.call-update) | async-done | bytes 131088 | tf_op jit(solution)/shard_map/reduce_scatter | solution.py:106
  84.0 24.2 %reduce-scatter.17.cloned.1.call-done = f32[8,8,512]{2,1,0:T(8,128)} async-done(((f32[32,8,512]{2,1,0:T(8,128)}), f32[8,8,512]{2,1,0:T(8,128)}) %reduce-scatter.17.cloned.1.call-update) | async-done | bytes 131088 | tf_op jit(solution)/shard_map/reduce_scatter | solution.py:106
  108.2 24.0 %reduce-scatter.19.cloned.1.call-done = f32[8,8,512]{2,1,0:T(8,128)} async-done(((f32[32,8,512]{2,1,0:T(8,128)}), f32[8,8,512]{2,1,0:T(8,128)}) %reduce-scatter.19.cloned.1.call-update) | async-done | bytes 131088 | tf_op jit(solution)/shard_map/reduce_scatter | solution.py:106
  132.3 24.0 %reduce-scatter.21.cloned.1.call-done = f32[8,8,512]{2,1,0:T(8,128)} async-done(((f32[32,8,512]{2,1,0:T(8,128)}), f32[8,8,512]{2,1,0:T(8,128)}) %reduce-scatter.21.cloned.1.call-update) | async-done | bytes 131088 | tf_op jit(solution)/shard_map/reduce_scatter | solution.py:106
  169.0 3.4 fusion.60
  173.5 3.3 add_select_fusion.14
  178.2 4.1 fusion.56
  185.5 5.1 add_select_fusion.13
  191.9 4.1 fusion.52
  199.2 5.8 add_select_fusion.12
  206.4 4.1 fusion.48
  213.7 7.1 add_select_fusion.11
  222.1 4.1 fusion.44
  229.3 8.5 %add_select_fusion.10 = f32[8,64,8,64]{3,2,1,0:T(8,128)S(1)} fusion(f32[8,8,64]{2,1,0:T(8,128)} %get-tuple-element.53, f32[8,64,8]{2,1,0:T(8,128)} %copy.40, f32[8,8,64]{2,1,0:T(8,128)} %get-tuple-element.37, f32[8,64,8]{2,1,0:T(8,128)} %bitcast.789, f32[8,8,64]{2,1,0:T(8,128)} %get-tuple-element.21, pred[8]{0:T(512)(128)(4,1)} %get-tuple-element.177, ...), kind=kLoop, calls=%fused_computation.37 | loop fusion | flops 9437184 | bytes 2588720 | tf_op jit(solution)/shard_map/jit(_where)/select_n | solution.py:51
  239.2 4.1 fusion.40
  246.4 10.0 %add_select_fusion.9 = f32[8,64,8,64]{3,2,1,0:T(8,128)S(1)} fusion(f32[8,8,64]{2,1,0:T(8,128)} %get-tuple-element.54, f32[8,64,8]{2,1,0:T(8,128)} %copy.41, f32[8,8,64]{2,1,0:T(8,128)} %get-tuple-element.38, f32[8,64,8]{2,1,0:T(8,128)} %bitcast.797, f32[8,8,64]{2,1,0:T(8,128)} %get-tuple-element.22, pred[8]{0:T(512)(128)(4,1)} %get-tuple-element.176, ...), kind=kLoop, calls=%fused_computation.36 | loop fusion | flops 11010048 | bytes 2670648 | tf_op jit(solution)/shard_map/jit(_where)/select_n | solution.py:51
  257.8 4.1 fusion.36
  263.4 5.2 fusion.62
  269.3 4.4 fusion.58
  274.3 4.4 fusion.54
  279.3 4.8 fusion.50
  284.7 4.4 fusion.46
  289.9 4.4 fusion.42
  294.9 4.2 fusion.38
  299.9 10.8 %add_select_fusion.8 = f32[8,64,8,64]{3,2,1,0:T(8,128)S(1)} fusion(f32[8,8,64]{2,1,0:T(8,128)} %get-tuple-element.55, f32[8,64,8]{2,1,0:T(8,128)S(1)} %copy-done.52, f32[8,8,64]{2,1,0:T(8,128)} %get-tuple-element.39, f32[8,64,8]{2,1,0:T(8,128)S(1)} %bitcast.804, f32[8,8,64]{2,1,0:T(8,128)} %get-tuple-element.23, pred[8]{0:T(512)(128)(4,1)S(1)} %copy-done.162, ...), kind=kLoop, calls=%fused_computation.35 | loop fusion | flops 12582912 | bytes 2752576 | tf_op jit(solution)/shard_map/jit(_where)/select_n | solution.py:51
  310.9 3.5 fusion.6
  319.9 5.8 all_gather.12
  325.7 13.8 %all_to_all.36 = bf16[32,8,512]{2,1,0:T(8,128)(2,1)S(1)} all-to-all(bf16[32,8,512]{2,1,0:T(8,128)(2,1)S(1)} %all_gather.12), channel_id=1, replica_groups=mesh['grp'=2,'tp'=4,'dp'=4] {'tp'}, dimensions={0} | all-to-all | bytes 524288 | tf_op jit(solution)/shard_map/all_to_all | solution.py:123
  342.8 8.0 %collective-permute-done.3 = f32[8,8,1024]{2,1,0:T(8,128)S(1)} collective-permute-done((f32[8,8,1024]{2,1,0:T(8,128)S(1)}, f32[8,8,1024]{2,1,0:T(8,128)S(1)}, u32[]{:S(2)}, u32[]{:S(2)}) %collective-permute-start.3) | collective-permute-done | bytes 262176 | tf_op jit(solution)/shard_map/ppermute | solution.py:90
  350.8 8.2 %collective-permute-done.4 = f32[8,8,1024]{2,1,0:T(8,128)S(1)} collective-permute-done((f32[8,8,1024]{2,1,0:T(8,128)S(1)}, f32[8,8,1024]{2,1,0:T(8,128)S(1)}, u32[]{:S(2)}, u32[]{:S(2)}) %collective-permute-start.4) | collective-permute-done | bytes 262176 | tf_op jit(solution)/shard_map/ppermute | solution.py:90
  359.0 8.2 %collective-permute-done.5 = f32[8,8,1024]{2,1,0:T(8,128)S(1)} collective-permute-done((f32[8,8,1024]{2,1,0:T(8,128)S(1)}, f32[8,8,1024]{2,1,0:T(8,128)S(1)}, u32[]{:S(2)}, u32[]{:S(2)}) %collective-permute-start.5) | collective-permute-done | bytes 262176 | tf_op jit(solution)/shard_map/ppermute | solution.py:90
  483.2 8.8 %add_select_fusion.17 = f32[1,8,64,512]{3,2,1,0:T(8,128)} fusion(f32[1,8,64,512]{3,2,1,0:T(8,128)S(1)} %copy-done.48, f32[1,8,64,512]{3,2,1,0:T(8,128)} %mul.1727, f32[1,8,64,512]{3,2,1,0:T(8,128)} %mul.1720, f32[1,8,64,512]{3,2,1,0:T(8,128)} %mul.1716, f32[1,8,64,512]{3,2,1,0:T(8,128)} %mul.1709, f32[1,8,64,512]{3,2,1,0:T(8,128)} %mul.1705, ...), kind=kLoop, calls=%fused_computation.140 | loop fusion | flops 12582912 | bytes 19267648 | tf_op jit(solution)/shard_map/jit(_where)/select_n | solution.py:51
  492.0 10.4 %all-reduce.1 = f32[32,8]{1,0:T(8,128)S(1)} all-reduce(f32[32,8]{1,0:T(8,128)S(1)} %copy-done.147), channel_id=12, replica_groups=mesh['grp'=2,'tp'=4,'dp'=4] {'dp'}, use_global_device_ids=true, to_apply=%region_13.15.clone | all-reduce | flops 256 | bytes 2048
  513.2 3.5 fusion.34
  517.5 5.0 fusion.32
  523.5 3.6 add_select_fusion.6
  527.1 4.1 fusion.30
  531.2 4.1 fusion.28
  538.5 4.6 add_select_fusion.5
  544.4 4.1 fusion.24
  551.7 6.2 add_select_fusion.4
  559.3 4.1 fusion.20
  566.6 7.1 add_select_fusion.3
  575.0 4.1 fusion.16
  582.2 8.4 %add_select_fusion.2 = f32[8,64,8,64]{3,2,1,0:T(8,128)S(1)} fusion(f32[8,8,64]{2,1,0:T(8,128)} %get-tuple-element.101, f32[8,64,8]{2,1,0:T(8,128)} %copy.49, f32[8,8,64]{2,1,0:T(8,128)} %get-tuple-element.85, f32[8,64,8]{2,1,0:T(8,128)} %bitcast.793, f32[8,8,64]{2,1,0:T(8,128)} %get-tuple-element.69, pred[8]{0:T(512)(128)(4,1)} %get-tuple-element.177, ...), kind=kLoop, calls=%fused_computation.29 | loop fusion | flops 9437184 | bytes 2588720 | tf_op jit(solution)/shard_map/jit(_where)/select_n | solution.py:51
  592.0 4.1 fusion.12
  597.7 9.9 %add_select_fusion.1 = f32[8,64,8,64]{3,2,1,0:T(8,128)S(1)} fusion(f32[8,8,64]{2,1,0:T(8,128)} %get-tuple-element.102, f32[8,64,8]{2,1,0:T(8,128)} %copy.50, f32[8,8,64]{2,1,0:T(8,128)} %get-tuple-element.86, f32[8,64,8]{2,1,0:T(8,128)} %bitcast.800, f32[8,8,64]{2,1,0:T(8,128)} %get-tuple-element.70, pred[8]{0:T(512)(128)(4,1)} %get-tuple-element.176, ...), kind=kLoop, calls=%fused_computation.28 | loop fusion | flops 11010048 | bytes 2670648 | tf_op jit(solution)/shard_map/jit(_where)/select_n | solution.py:51
  608.9 4.1 fusion.8
  616.8 5.2 fusion.26
  622.7 4.4 fusion.22
  627.7 4.4 fusion.18
  632.9 4.6 fusion.14
  638.1 4.2 fusion.10
  643.1 10.7 %add_select_fusion = f32[8,64,8,64]{3,2,1,0:T(8,128)S(1)} fusion(f32[8,8,64]{2,1,0:T(8,128)} %get-tuple-element.103, f32[8,64,8]{2,1,0:T(8,128)} %copy.51, f32[8,8,64]{2,1,0:T(8,128)} %get-tuple-element.87, f32[8,64,8]{2,1,0:T(8,128)S(1)} %bitcast.806, f32[8,8,64]{2,1,0:T(8,128)} %get-tuple-element.71, pred[8]{0:T(512)(128)(4,1)S(1)} %copy-done.163, ...), kind=kLoop, calls=%fused_computation.27 | loop fusion | flops 12582912 | bytes 2752576 | tf_op jit(solution)/shard_map/jit(_where)/select_n | solution.py:51
  653.9 3.5 fusion.4
  662.9 6.2 all_gather.14
  669.1 4.4 all-to-all-start.1
  727.7 8.3 %add_select_fusion.16 = f32[1,8,64,512]{3,2,1,0:T(8,128)S(1)} fusion(f32[1,8,64,512]{3,2,1,0:T(8,128)} %mul.1819, f32[1,8,64,512]{3,2,1,0:T(8,128)} %mul.1815, f32[1,8,64,512]{3,2,1,0:T(8,128)} %mul.1808, f32[1,8,64,512]{3,2,1,0:T(8,128)} %mul.1804, f32[1,8,64,512]{3,2,1,0:T(8,128)} %mul.1797, f32[1,8,64,512]{3,2,1,0:T(8,128)} %mul.1793, ...), kind=kLoop, calls=%fused_computation.139 | loop fusion | flops 12582912 | bytes 19267648 | tf_op jit(solution)/shard_map/jit(_where)/select_n | solution.py:51
  738.6 3.7 fusion.67
  (663 shorter events, 295.4 us)
Async XLA Ops:
  8.0 31.0 %copy-start.172 = (bf16[2,1024,512]{2,1,0:T(8,128)(2,1)S(1)}, bf16[2,1024,512]{2,1,0:T(8,128)(2,1)}, u32[]{:S(2)}) copy-start(bf16[2,1024,512]{2,1,0:T(8,128)(2,1)} %param.21) | copy-start | bytes 6291460
  8.0 64.7 %reduce-scatter.13.cloned.1.call-start = ((), (), s32[]{:S(2)}) async-start(), calls=%async_computation.14 | async-start | bytes 655360 | tf_op jit(solution)/shard_map/reduce_scatter | solution.py:106
  9.1 11.4 %collective-permute-start = (f32[8,8,1024]{2,1,0:T(8,128)S(1)}, f32[8,8,1024]{2,1,0:T(8,128)S(1)}, u32[]{:S(2)}, u32[]{:S(2)}) collective-permute-start(f32[8,8,1024]{2,1,0:T(8,128)S(1)} %convert_element_type.15), channel_id=1, source_target_pairs={{0,4},{4,8},{8,12},{12,0},{1,5},{5,9},{9,13},{13,1},{2,6},{6,10},{... | collective-permute-start | bytes 786440 | tf_op jit(solution)/shard_map/ppermute | solution.py:90
  20.6 9.3 %collective-permute-start.1 = (f32[8,8,1024]{2,1,0:T(8,128)S(1)}, f32[8,8,1024]{2,1,0:T(8,128)S(1)}, u32[]{:S(2)}, u32[]{:S(2)}) collective-permute-start(f32[8,8,1024]{2,1,0:T(8,128)S(1)} %collective-permute-done), channel_id=1, source_target_pairs={{0,4},{4,8},{8,12},{12,0},{1,5},{5,9},{9,13},{13,1},{2,6},{6,10},{... | collective-permute-start | bytes 786440 | tf_op jit(solution)/shard_map/ppermute | solution.py:90
  29.8 8.4 %collective-permute-start.2 = (f32[8,8,1024]{2,1,0:T(8,128)S(1)}, f32[8,8,1024]{2,1,0:T(8,128)S(1)}, u32[]{:S(2)}, u32[]{:S(2)}) collective-permute-start(f32[8,8,1024]{2,1,0:T(8,128)S(1)} %collective-permute-done.1), channel_id=1, source_target_pairs={{0,4},{4,8},{8,12},{12,0},{1,5},{5,9},{9,13},{13,1},{2,6},{6,10},{... | collective-permute-start | bytes 786440 | tf_op jit(solution)/shard_map/ppermute | solution.py:90
  40.3 43.7 %reduce-scatter.15.cloned.1.call-start = ((), (), s32[]{:S(2)}) async-start(), calls=%async_computation.15 | async-start | bytes 655360 | tf_op jit(solution)/shard_map/reduce_scatter | solution.py:106
  43.0 65.2 %reduce-scatter.17.cloned.1.call-start = ((), (), s32[]{:S(2)}) async-start(), calls=%async_computation.16 | async-start | bytes 655360 | tf_op jit(solution)/shard_map/reduce_scatter | solution.py:106
  44.3 87.9 %reduce-scatter.19.cloned.1.call-start = ((), (), s32[]{:S(2)}) async-start(), calls=%async_computation.17 | async-start | bytes 655360 | tf_op jit(solution)/shard_map/reduce_scatter | solution.py:106
  47.1 109.2 %reduce-scatter.21.cloned.1.call-start = ((), (), s32[]{:S(2)}) async-start(), calls=%async_computation.18 | async-start | bytes 655360 | tf_op jit(solution)/shard_map/reduce_scatter | solution.py:106
  48.5 270.4 %reduce-scatter.23.cloned.1.call-start = ((), (), s32[]{:S(2)}) async-start(), calls=%async_computation.19 | async-start | bytes 655360 | tf_op jit(solution)/shard_map/reduce_scatter | solution.py:106
  51.0 288.5 %all-gather.5.cloned.1.call-start = ((), (), s32[]{:S(2)}) async-start(), calls=%async_computation.26 | async-start | bytes 5242880 | tf_op jit(solution)/shard_map/all_gather | solution.py:127
  54.3 448.2 %reduce-scatter.25.cloned.1.call-start = ((), (), s32[]{:S(2)}) async-start(), calls=%async_computation.20 | async-start | bytes 655360 | tf_op jit(solution)/shard_map/reduce_scatter | solution.py:106
  72.7 85.6 %copy-start.156 = (f32[8,8]{1,0:T(8,128)}, f32[8,8]{1,0:T(8,128)S(1)}, u32[]{:S(2)}) copy-start(f32[8,8]{1,0:T(8,128)S(1)} %fusion.123) | copy-start | bytes 772
  246.4 11.3 %copy-start.99 = (f32[8,1,8,64]{3,2,1,0:T(8,128)S(1)}, f32[8,1,8,64]{3,2,1,0:T(8,128)}, u32[]{:S(2)}) copy-start(f32[8,1,8,64]{3,2,1,0:T(8,128)} %get-tuple-element.135) | copy-start | bytes 49156
  263.4 10.8 %copy-start.13 = (f32[8,64,8,64]{3,2,1,0:T(8,128)S(1)}, f32[8,64,8,64]{3,2,1,0:T(8,128)}, u32[]{:S(2)}) copy-start(f32[8,64,8,64]{3,2,1,0:T(8,128)} %copy-done.12) | copy-start | bytes 3145732
  273.6 10.4 %copy-start.72 = (f32[8,8,1,64]{3,2,1,0:T(1,128)}, f32[8,8,1,64]{3,2,1,0:T(1,128)S(1)}, u32[]{:S(2)}) copy-start(f32[8,8,1,64]{3,2,1,0:T(1,128)S(1)} %fusion.58) | copy-start | bytes 49156
  274.3 10.4 %copy-start.20 = (f32[8,64,8,64]{3,2,1,0:T(8,128)S(1)}, f32[8,64,8,64]{3,2,1,0:T(8,128)}, u32[]{:S(2)}) copy-start(f32[8,64,8,64]{3,2,1,0:T(8,128)} %copy-done.19) | copy-start | bytes 3145732
  278.6 10.4 %copy-start.74 = (f32[8,8,1,64]{3,2,1,0:T(1,128)}, f32[8,8,1,64]{3,2,1,0:T(1,128)S(1)}, u32[]{:S(2)}) copy-start(f32[8,8,1,64]{3,2,1,0:T(1,128)S(1)} %fusion.54) | copy-start | bytes 49156
  279.3 10.4 %copy-start.2 = (f32[8,64,8,64]{3,2,1,0:T(8,128)S(1)}, f32[8,64,8,64]{3,2,1,0:T(8,128)}, u32[]{:S(2)}) copy-start(f32[8,64,8,64]{3,2,1,0:T(8,128)} %copy-done.1) | copy-start | bytes 3145732
  294.2 16.5 %copy-start.86 = (f32[8,8,1,64]{3,2,1,0:T(1,128)}, f32[8,8,1,64]{3,2,1,0:T(1,128)S(1)}, u32[]{:S(2)}) copy-start(f32[8,8,1,64]{3,2,1,0:T(1,128)S(1)} %fusion.42) | copy-start | bytes 49156
  299.9 10.9 %copy-start.94 = (f32[8,1,8,64]{3,2,1,0:T(8,128)S(1)}, f32[8,1,8,64]{3,2,1,0:T(8,128)}, u32[]{:S(2)}) copy-start(f32[8,1,8,64]{3,2,1,0:T(8,128)} %get-tuple-element.151) | copy-start | bytes 49156
  317.3 22.2 %copy-start.65 = (bf16[8,8,1024]{2,1,0:T(8,128)(2,1)S(1)}, bf16[8,8,1024]{2,1,0:T(8,128)(2,1)}, u32[]{:S(2)}) copy-start(bf16[8,8,1024]{2,1,0:T(8,128)(2,1)} %param.15) | copy-start | bytes 393220
  342.5 26.0 %copy-start.50 = (f32[8,8,1024]{2,1,0:T(8,128)}, f32[8,8,1024]{2,1,0:T(8,128)S(1)}, u32[]{:S(2)}) copy-start(f32[8,8,1024]{2,1,0:T(8,128)S(1)} %fusion.64) | copy-start | bytes 786436
  342.6 25.8 %copy-start.161 = (f32[1,1024]{1,0:T(1,128)S(1)}, f32[1,1024]{1,0:T(1,128)}, u32[]{:S(2)}) copy-start(f32[1,1024]{1,0:T(1,128)} %get-tuple-element.159) | copy-start | bytes 12292
  342.6 26.0 %copy-start.173 = (bf16[2,1024,512]{2,1,0:T(8,128)(2,1)S(1)}, bf16[2,1024,512]{2,1,0:T(8,128)(2,1)}, u32[]{:S(2)}) copy-start(bf16[2,1024,512]{2,1,0:T(8,128)(2,1)} %param.21) | copy-start | bytes 6291460
  342.6 8.2 %collective-permute-start.3 = (f32[8,8,1024]{2,1,0:T(8,128)S(1)}, f32[8,8,1024]{2,1,0:T(8,128)S(1)}, u32[]{:S(2)}, u32[]{:S(2)}) collective-permute-start(f32[8,8,1024]{2,1,0:T(8,128)S(1)} %fusion.64), channel_id=1, source_target_pairs={{0,4},{4,8},{8,12},{12,0},{1,5},{5,9},{9,13},{13,1},{2,6},{6,10},{... | collective-permute-start | bytes 786440 | tf_op jit(solution)/shard_map/ppermute | solution.py:90
  350.8 8.2 %collective-permute-start.4 = (f32[8,8,1024]{2,1,0:T(8,128)S(1)}, f32[8,8,1024]{2,1,0:T(8,128)S(1)}, u32[]{:S(2)}, u32[]{:S(2)}) collective-permute-start(f32[8,8,1024]{2,1,0:T(8,128)S(1)} %collective-permute-done.3), channel_id=1, source_target_pairs={{0,4},{4,8},{8,12},{12,0},{1,5},{5,9},{9,13},{13,1},{2,6},{6,10},{... | collective-permute-start | bytes 786440 | tf_op jit(solution)/shard_map/ppermute | solution.py:90
  359.0 8.2 %collective-permute-start.5 = (f32[8,8,1024]{2,1,0:T(8,128)S(1)}, f32[8,8,1024]{2,1,0:T(8,128)S(1)}, u32[]{:S(2)}, u32[]{:S(2)}) collective-permute-start(f32[8,8,1024]{2,1,0:T(8,128)S(1)} %collective-permute-done.4), channel_id=1, source_target_pairs={{0,4},{4,8},{8,12},{12,0},{1,5},{5,9},{9,13},{13,1},{2,6},{6,10},{... | collective-permute-start | bytes 786440 | tf_op jit(solution)/shard_map/ppermute | solution.py:90
  369.9 132.7 %reduce-scatter.27.cloned.1.call-start = ((), (), s32[]{:S(2)}) async-start(), calls=%async_computation.21 | async-start | bytes 655360 | tf_op jit(solution)/shard_map/reduce_scatter | solution.py:106
  372.4 130.2 %reduce-scatter.29.cloned.1.call-start = ((), (), s32[]{:S(2)}) async-start(), calls=%async_computation.22 | async-start | bytes 655360 | tf_op jit(solution)/shard_map/reduce_scatter | solution.py:106
  374.9 127.7 %reduce-scatter.31.cloned.1.call-start = ((), (), s32[]{:S(2)}) async-start(), calls=%async_computation.23 | async-start | bytes 655360 | tf_op jit(solution)/shard_map/reduce_scatter | solution.py:106
  377.5 125.1 %reduce-scatter.33.cloned.1.call-start = ((), (), s32[]{:S(2)}) async-start(), calls=%async_computation.24 | async-start | bytes 655360 | tf_op jit(solution)/shard_map/reduce_scatter | solution.py:106
  380.0 281.8 %reduce-scatter.35.cloned.1.call-start = ((), (), s32[]{:S(2)}) async-start(), calls=%async_computation.25 | async-start | bytes 655360 | tf_op jit(solution)/shard_map/reduce_scatter | solution.py:106
  382.6 356.0 %all-gather.7.cloned.1.call-start = ((), (), s32[]{:S(2)}) async-start(), calls=%async_computation.27 | async-start | bytes 5242880 | tf_op jit(solution)/shard_map/all_gather | solution.py:127
  466.4 12.2 %copy-start.114 = (f32[8,1,8,64]{3,2,1,0:T(8,128)S(1)}, f32[8,1,8,64]{3,2,1,0:T(8,128)}, u32[]{:S(2)}) copy-start(f32[8,1,8,64]{3,2,1,0:T(8,128)} %get-tuple-element.60) | copy-start | bytes 49156
  466.4 12.9 %copy-start.122 = (f32[8,1,8,64]{3,2,1,0:T(8,128)S(1)}, f32[8,1,8,64]{3,2,1,0:T(8,128)}, u32[]{:S(2)}) copy-start(f32[8,1,8,64]{3,2,1,0:T(8,128)} %get-tuple-element.44) | copy-start | bytes 49156
  466.4 13.8 %copy-start.113 = (f32[8,1,8,64]{3,2,1,0:T(8,128)S(1)}, f32[8,1,8,64]{3,2,1,0:T(8,128)}, u32[]{:S(2)}) copy-start(f32[8,1,8,64]{3,2,1,0:T(8,128)} %get-tuple-element.61) | copy-start | bytes 49156
  466.4 13.9 %copy-start.121 = (f32[8,1,8,64]{3,2,1,0:T(8,128)S(1)}, f32[8,1,8,64]{3,2,1,0:T(8,128)}, u32[]{:S(2)}) copy-start(f32[8,1,8,64]{3,2,1,0:T(8,128)} %get-tuple-element.45) | copy-start | bytes 49156
  466.4 14.8 %copy-start.112 = (f32[8,1,8,64]{3,2,1,0:T(8,128)S(1)}, f32[8,1,8,64]{3,2,1,0:T(8,128)}, u32[]{:S(2)}) copy-start(f32[8,1,8,64]{3,2,1,0:T(8,128)} %get-tuple-element.62) | copy-start | bytes 49156
  466.4 14.8 %copy-start.120 = (f32[8,1,8,64]{3,2,1,0:T(8,128)S(1)}, f32[8,1,8,64]{3,2,1,0:T(8,128)}, u32[]{:S(2)}) copy-start(f32[8,1,8,64]{3,2,1,0:T(8,128)} %get-tuple-element.46) | copy-start | bytes 49156
  466.5 15.7 %copy-start.111 = (f32[8,1,8,64]{3,2,1,0:T(8,128)S(1)}, f32[8,1,8,64]{3,2,1,0:T(8,128)}, u32[]{:S(2)}) copy-start(f32[8,1,8,64]{3,2,1,0:T(8,128)} %get-tuple-element.47) | copy-start | bytes 49156
  466.5 15.8 %copy-start.119 = (f32[8,1,8,64]{3,2,1,0:T(8,128)S(1)}, f32[8,1,8,64]{3,2,1,0:T(8,128)}, u32[]{:S(2)}) copy-start(f32[8,1,8,64]{3,2,1,0:T(8,128)} %get-tuple-element.31) | copy-start | bytes 49156
  466.5 16.7 %copy-start.48 = (f32[1,8,64,512]{3,2,1,0:T(8,128)S(1)}, f32[1,8,64,512]{3,2,1,0:T(8,128)}, u32[]{:S(2)}) copy-start(f32[1,8,64,512]{3,2,1,0:T(8,128)} %mul.1731) | copy-start | bytes 3145732
  483.2 19.5 %copy-start.168 = (f32[1,512]{1,0:T(1,128)S(1)}, f32[1,512]{1,0:T(1,128)}, u32[]{:S(2)}) copy-start(f32[1,512]{1,0:T(1,128)} %get-tuple-element.168) | copy-start | bytes 6148
  597.7 11.3 %copy-start.98 = (f32[8,1,8,64]{3,2,1,0:T(8,128)S(1)}, f32[8,1,8,64]{3,2,1,0:T(8,128)}, u32[]{:S(2)}) copy-start(f32[8,1,8,64]{3,2,1,0:T(8,128)} %get-tuple-element.111) | copy-start | bytes 49156
  616.8 10.8 %copy-start.22 = (f32[8,64,8,64]{3,2,1,0:T(8,128)S(1)}, f32[8,64,8,64]{3,2,1,0:T(8,128)}, u32[]{:S(2)}) copy-start(f32[8,64,8,64]{3,2,1,0:T(8,128)} %copy-done.21) | copy-start | bytes 3145732
  627.7 10.4 %copy-start.8 = (f32[8,64,8,64]{3,2,1,0:T(8,128)S(1)}, f32[8,64,8,64]{3,2,1,0:T(8,128)}, u32[]{:S(2)}) copy-start(f32[8,64,8,64]{3,2,1,0:T(8,128)} %copy-done.7) | copy-start | bytes 3145732
  632.7 10.3 %copy-start.25 = (f32[8,8,1,64]{1,3,0,2:T(8,128)S(1)}, f32[8,8,1,64]{1,3,0,2:T(8,128)}, u32[]{:S(2)}) copy-start(f32[8,8,1,64]{1,3,0,2:T(8,128)} %copy.112) | copy-start | bytes 49156
  632.7 10.3 %copy-start.29 = (f32[8,64,8]{2,1,0:T(8,128)S(1)}, f32[8,64,8]{2,1,0:T(8,128)}, u32[]{:S(2)}) copy-start(f32[8,64,8]{2,1,0:T(8,128)} %copy.47) | copy-start | bytes 49156
  632.7 10.3 %copy-start.31 = (f32[8,8,1,64]{1,3,0,2:T(8,128)S(1)}, f32[8,8,1,64]{1,3,0,2:T(8,128)}, u32[]{:S(2)}) copy-start(f32[8,8,1,64]{1,3,0,2:T(8,128)} %copy.117) | copy-start | bytes 49156
  632.7 10.3 %copy-start.35 = (f32[8,64,8]{2,1,0:T(8,128)S(1)}, f32[8,64,8]{2,1,0:T(8,128)}, u32[]{:S(2)}) copy-start(f32[8,64,8]{2,1,0:T(8,128)} %copy.48) | copy-start | bytes 49156
  632.7 10.3 %copy-start.37 = (f32[8,8,1,64]{1,3,0,2:T(8,128)S(1)}, f32[8,8,1,64]{1,3,0,2:T(8,128)}, u32[]{:S(2)}) copy-start(f32[8,8,1,64]{1,3,0,2:T(8,128)} %copy.122) | copy-start | bytes 49156
  632.7 10.3 %copy-start.42 = (f32[8,64,8]{2,1,0:T(8,128)S(1)}, f32[8,64,8]{2,1,0:T(8,128)}, u32[]{:S(2)}) copy-start(f32[8,64,8]{2,1,0:T(8,128)} %copy.49) | copy-start | bytes 49156
  632.7 10.3 %copy-start.43 = (f32[8,8,1,64]{1,3,0,2:T(8,128)S(1)}, f32[8,8,1,64]{1,3,0,2:T(8,128)}, u32[]{:S(2)}) copy-start(f32[8,8,1,64]{1,3,0,2:T(8,128)} %copy.127) | copy-start | bytes 49156
  632.7 10.3 %copy-start.46 = (f32[8,64,8]{2,1,0:T(8,128)S(1)}, f32[8,64,8]{2,1,0:T(8,128)}, u32[]{:S(2)}) copy-start(f32[8,64,8]{2,1,0:T(8,128)} %copy.50) | copy-start | bytes 49156
  632.7 10.3 %copy-start.47 = (f32[8,8,1,64]{1,3,0,2:T(8,128)S(1)}, f32[8,8,1,64]{1,3,0,2:T(8,128)}, u32[]{:S(2)}) copy-start(f32[8,8,1,64]{1,3,0,2:T(8,128)} %copy.132) | copy-start | bytes 49156
  632.8 10.3 %copy-start.54 = (f32[8,8,1,64]{1,3,0,2:T(8,128)S(1)}, f32[8,8,1,64]{1,3,0,2:T(8,128)}, u32[]{:S(2)}) copy-start(f32[8,8,1,64]{1,3,0,2:T(8,128)} %copy.137) | copy-start | bytes 49156
  632.8 10.3 %copy-start.56 = (f32[8,8,64]{2,1,0:T(8,128)S(1)}, f32[8,8,64]{2,1,0:T(8,128)}, u32[]{:S(2)}) copy-start(f32[8,8,64]{2,1,0:T(8,128)} %get-tuple-element.81) | copy-start | bytes 49156
  632.8 10.3 %copy-start.58 = (f32[8,8,64]{2,1,0:T(8,128)S(1)}, f32[8,8,64]{2,1,0:T(8,128)}, u32[]{:S(2)}) copy-start(f32[8,8,64]{2,1,0:T(8,128)} %get-tuple-element.65) | copy-start | bytes 49156
  632.8 10.3 %copy-start.60 = (f32[8,8,64]{2,1,0:T(8,128)S(1)}, f32[8,8,64]{2,1,0:T(8,128)}, u32[]{:S(2)}) copy-start(f32[8,8,64]{2,1,0:T(8,128)} %get-tuple-element.98) | copy-start | bytes 49156
  632.8 10.3 %copy-start.62 = (f32[8,8,64]{2,1,0:T(8,128)S(1)}, f32[8,8,64]{2,1,0:T(8,128)}, u32[]{:S(2)}) copy-start(f32[8,8,64]{2,1,0:T(8,128)} %get-tuple-element.82) | copy-start | bytes 49156
  637.4 16.4 %copy-start.88 = (f32[8,8,1,64]{3,2,1,0:T(1,128)}, f32[8,8,1,64]{3,2,1,0:T(1,128)S(1)}, u32[]{:S(2)}) copy-start(f32[8,8,1,64]{3,2,1,0:T(1,128)S(1)} %fusion.14) | copy-start | bytes 49156
  643.1 10.8 %copy-start.95 = (f32[8,1,8,64]{3,2,1,0:T(8,128)S(1)}, f32[8,1,8,64]{3,2,1,0:T(8,128)}, u32[]{:S(2)}) copy-start(f32[8,1,8,64]{3,2,1,0:T(8,128)} %get-tuple-element.127) | copy-start | bytes 49156
  669.1 68.5 %all-to-all-start.1 = ((bf16[32,8,512]{2,1,0:T(8,128)(2,1)}), bf16[32,8,512]{2,1,0:T(8,128)(2,1)}, u32[]{:S(2)}, u32[]{:S(2)}) async-start(bf16[32,8,512]{2,1,0:T(8,128)(2,1)} %all_gather.14), calls=%async_computation.13 | async-start | bytes 524288 | tf_op jit(solution)/shard_map/all_to_all | solution.py:123
  (135 other events, 723.3 us)
Sparse Core Ops, SparseCore 0:
  40.4 19.4 reduce-scatter.12
  62.4 21.6 reduce-scatter.14
  86.5 21.6 reduce-scatter.16
  110.6 21.6 reduce-scatter.18
  134.6 21.6 reduce-scatter.20
  158.6 21.6 reduce-scatter.22
  370.0 18.9 reduce-scatter.24
  391.4 21.6 reduce-scatter.26
  415.6 21.6 reduce-scatter.28
  439.6 21.6 reduce-scatter.30
  463.8 21.6 reduce-scatter.32
  487.9 21.6 reduce-scatter.34
Sparse Core Ops, SparseCore 1:
  54.4 78.3 all-gather.4
  384.7 77.8 all-gather.6
